TPU v7x, 128 devices: a whole 4x4x4 slice. The times are simulated.
128 devices in a mesh: fs: 16 (over z, y), tp: 8 (over x, core).
Axes of the slice: x: 4, y: 4, z: 4, core: 2. Of those that a mesh axis runs over, the one named last changes fastest.
Arguments:
- weights_in: float32 [2, 2048, 5632], P(None, 'fs', 'tp'), may hold values from -6 to 6
- weights_mix: float32 [2048, 2048], P('fs', 'tp'), may hold values from -6 to 6
- momentum_in: float32 [2, 2048, 5632], P(None, 'fs', 'tp'), may hold values from -5 to 5
- momentum_mix: float32 [2048, 2048], P('fs', 'tp'), may hold values from -5 to 5
- grads_in: float32 [2, 2048, 5632], P(None, 'fs', 'tp'), may hold values from -5 to 5
- grads_mix: float32 [2048, 2048], P('fs', 'tp'), may hold values from -5 to 5
Outputs:
- momentum_in_next: float32 [2, 2048, 5632], P(None, 'fs', 'tp')
- momentum_mix_next: float32 [2048, 2048], P('fs', 'tp')
- weights_in_next: float32 [2, 2048, 5632], P(None, 'fs', 'tp')
- weights_mix_next: float32 [2048, 2048], P('fs', 'tp')
- update_in: float32 [2, 2048, 5632], P(None, 'fs', 'tp')
- update_mix: float32 [2048, 2048], P('fs', 'tp')
All inputs are finite; a program needn't handle non-finite values.
Results may differ from a plain program's by a relative error of at most 0.0003.
Values sent between devices are 32-bit elements; how exact they have to be, the bound alone decides.
No kernel may reach another device: no remote copies, remote signals or barrier semaphores. Data moves between devices by JAX's collectives and lax.ppermute only.
A program may use at most 128 MiB of HBM per device.

v0:
```python
import math
import jax
import jax.numpy as jnp
from jax import lax
from jax.sharding import PartitionSpec as P

D = 2048
FF = 5632
ITERS = 3
A_COEF = 3.4445
B_COEF = -4.775
C_COEF = 2.0315
MOMENTUM_DECAY = 0.95
STEP_RATE = 0.02
HIGH = lax.Precision.HIGHEST


def gather_turned(arrays, axis, dims):
    turned = [jnp.moveaxis(a, dim, 0) for a, dim in zip(arrays, dims)]
    both = jnp.concatenate([t.reshape(len(t), -1) for t in turned], axis=1)
    result, at, gathered = (lax.all_gather(both, axis, axis=0, tiled=True), 0, [])
    for t, dim in zip(turned, dims):
        share = result[:, at : at + t[0].size].reshape(-1, *t.shape[1:])
        gathered.append(jnp.moveaxis(share, 0, dim))
        at += t[0].size
    return tuple(gathered)


def rows_for(lines, peers):
    spare = -lines.shape[0] % peers
    if not spare:
        return lines
    return jnp.concatenate([lines, jnp.zeros((spare, *lines.shape[1:]), lines.dtype)])


def sum_by_parts(shard, axis):
    lines = shard.reshape(-1, *shard.shape[1:][-1:])
    own = lax.psum_scatter(
        rows_for(lines, lax.axis_size(axis)), axis, scatter_dimension=0, tiled=True
    )
    whole = lax.all_gather(own, axis).reshape(-1, *lines.shape[1:])
    return lax.slice_in_dim(whole, 0, len(lines)).reshape(shard.shape)


def scale_from(summed):
    return (0.5 * lax.rsqrt(jnp.maximum(summed / D, 1.0)))[:, None, None]


def block_trace(shard, row_start, col_start):
    row_ids = row_start + lax.iota(jnp.int32, shard.shape[1])[:, None]
    col_ids = col_start + lax.iota(jnp.int32, shard.shape[2])[None, :]
    return jnp.sum(jnp.where((row_ids == col_ids)[None], shard, 0.0), axis=(1, 2))


def local(weights_in, weights_mix, momentum_in, momentum_mix, grads_in, grads_mix):
    fs_pos = lax.axis_index("fs")
    tp_pos = lax.axis_index("tp")
    moment_in = MOMENTUM_DECAY * momentum_in + grads_in
    moment_mix = MOMENTUM_DECAY * momentum_mix + grads_mix
    local_in = moment_in
    local_mix = moment_mix[None]
    row_count = local_in.shape[1]
    block_width = local_mix.shape[2]
    for iteration in range(ITERS):
        cols_in, cols_mix = gather_turned((local_in, local_mix), "fs", (1, 1))
        partial_value = jnp.concatenate(
            [
                jnp.einsum("krc,ksc->krs", local_in, cols_in, precision=HIGH),
                jnp.einsum("krc,ksc->krs", local_mix, cols_mix, precision=HIGH),
            ]
        )
        gram_rows = sum_by_parts(partial_value, "tp")
        gram_block = lax.dynamic_slice_in_dim(gram_rows, tp_pos * block_width, block_width, 2)
        if iteration == 0:
            traces = block_trace(gram_block, fs_pos * row_count, tp_pos * block_width)
            scaling = scale_from(lax.psum(traces, ("fs", "tp")))
        factor = scaling if iteration == 0 else jnp.ones_like(scaling)
        gram_cols = lax.all_gather(gram_block, "fs", axis=1, tiled=True)
        square = jnp.einsum("krs,ksc->krc", gram_rows, gram_cols, precision=HIGH)
        poly_mat = factor**2 * B_COEF * gram_block + factor**4 * C_COEF * square
        poly_rows = lax.all_gather(poly_mat, "tp", axis=2, tiled=True)
        local_in = factor[:2] * (
            A_COEF * local_in + jnp.einsum("krs,ksc->krc", poly_rows[:2], cols_in, precision=HIGH)
        )
        local_mix = factor[2:] * (
            A_COEF * local_mix + jnp.einsum("krs,ksc->krc", poly_rows[2:], cols_mix, precision=HIGH)
        )
    step_in = local_in * math.sqrt(max(D, FF))
    step_mix = local_mix[0] * math.sqrt(D)
    return (
        moment_in,
        moment_mix,
        weights_in - STEP_RATE * step_in,
        weights_mix - STEP_RATE * step_mix,
        step_in,
        step_mix,
    )


def solution(mesh):
    in_specs = (
        P(None, "fs", "tp"),
        P("fs", "tp"),
        P(None, "fs", "tp"),
        P("fs", "tp"),
        P(None, "fs", "tp"),
        P("fs", "tp"),
    )
    out_specs = (
        P(None, "fs", "tp"),
        P("fs", "tp"),
        P(None, "fs", "tp"),
        P("fs", "tp"),
        P(None, "fs", "tp"),
        P("fs", "tp"),
    )
    return jax.shard_map(local, mesh=mesh, in_specs=in_specs, out_specs=out_specs, check_vma=False)
```

profile of v0, /device:TPU:1, one launch (start us, length us, event | category | flops | bytes accessed | tf_op | source)
XLA Modules:
  0.0 954.7 jit_solution(4597433947635089846)
XLA Ops:
  7.2 0.0 all-gather.16.cloned.1.call-start
  7.2 1.0 multiply_add_fusion.1
  8.2 0.1 copy.12
  8.3 1.4 multiply_add_fusion
  9.7 1.1 pad_maximum_fusion.3
  10.8 0.0 reduce-scatter.4.cloned.1.call-start
  10.9 105.9 %all-gather.16.cloned.1.call-done = f32[2048,1664]{0,1:T(8,128)} async-done(((f32[128,1664]{0,1:T(8,128)}), f32[2048,1664]{0,1:T(8,128)}) %all-gather.16.cloned.1.call-update) | async-done | bytes 13631504 | tf_op jit(solution)/shard_map/all_gather | solution.py:21
  116.8 10.4 %slice.58 = f32[2048,1408]{0,1:T(8,128)} slice(f32[2048,1664]{0,1:T(8,128)} %all-gather.16.cloned.1.call-done), slice={[0:2048], [0:1408]} | slice | bytes 23068672 | tf_op jit(solution)/shard_map/slice | solution.py:23
  127.2 9.2 fusion.25
  136.4 2.8 convolution_bitcast_fusion.2
  139.2 1.9 pad_maximum_fusion
  141.2 0.0 all-gather.34.cloned.1.call-start
  141.2 33.7 %reduce-scatter.4.cloned.1.call-done = f32[48,2048]{1,0:T(8,128)} async-done(((f32[384,2048]{1,0:T(8,128)}), f32[48,2048]{1,0:T(8,128)}) %reduce-scatter.4.cloned.1.call-update) | async-done | bytes 393232 | tf_op jit(solution)/shard_map/reduce_scatter | solution.py:38
  174.9 0.0 all-gather.18.cloned.1.call-start
  175.0 0.1 broadcast_compare_fusion
  175.1 31.3 %all-gather.34.cloned.1.call-done = f32[384,2048]{1,0:T(8,128)} async-done(((f32[48,2048]{1,0:T(8,128)}), f32[384,2048]{1,0:T(8,128)}) %all-gather.34.cloned.1.call-update) | async-done | bytes 3145744 | tf_op jit(solution)/shard_map/all_gather | solution.py:41
  206.4 1.8 select_reduce_fusion
  208.2 0.0 all-gather.20.cloned.1.call-start
  208.3 67.5 %psum.7 = f32[3]{0:T(128)S(1)} all-reduce(f32[3]{0:T(128)S(1)} %get-tuple-element.8), channel_id=1, replica_groups=mesh['fs'=16,'tp'=8] {'fs','tp'}, use_global_device_ids=true, to_apply=%region_2.3 | all-reduce | flops 3 | bytes 24 | tf_op jit(solution)/shard_map/psum | solution.py:76
  275.8 8.2 fusion.10
  284.1 0.2 all-gather.22.cloned.1.call-start
  284.3 0.6 slice.48
  284.9 23.8 %all-gather.20.cloned.1.call-done = f32[3,128,2048]{2,1,0:T(8,128)} async-done(((f32[3,128,256]{2,1,0:T(8,128)}), f32[3,128,2048]{2,1,0:T(8,128)}) %all-gather.20.cloned.1.call-update) | async-done | bytes 3145744 | tf_op jit(solution)/shard_map/all_gather | solution.py:81
  308.7 4.8 fusion.16
  313.5 0.1 copy.13
  313.6 13.0 %fusion.9 = f32[2,128,704]{1,2,0:T(8,128)S(1)} fusion(f32[3,128,2048]{2,1,0:T(8,128)} %all-gather.20.cloned.1.call-done, f32[2,2048,704]{1,2,0:T(8,128)} %bitcast.65, f32[2,128,704]{1,2,0:T(8,128)S(1)} %multiply_add_fusion, f32[2]{0:T(128)S(1)} %bitcast.82), kind=kOutput, calls=%fused_computation.18 | convolution fusion | flops 4429725696 | bytes 16121864 | tf_op jit(solution)/shard_map/krs,ksc->krc/dot_general | solution.py:83
  326.6 1.0 pad_maximum_fusion.4
  327.6 0.3 reduce-scatter.6.cloned.1.call-start
  327.9 102.1 %all-gather.22.cloned.1.call-done = f32[2048,1664]{0,1:T(8,128)} async-done(((f32[128,1664]{0,1:T(8,128)}), f32[2048,1664]{0,1:T(8,128)}) %all-gather.22.cloned.1.call-update) | async-done | bytes 13631504 | tf_op jit(solution)/shard_map/all_gather | solution.py:21
  429.9 10.4 %slice.61 = f32[2048,1408]{0,1:T(8,128)} slice(f32[2048,1664]{0,1:T(8,128)} %all-gather.22.cloned.1.call-done), slice={[0:2048], [0:1408]} | slice | bytes 23068672 | tf_op jit(solution)/shard_map/slice | solution.py:23
  440.3 9.2 fusion.26
  449.5 2.8 convolution_bitcast_fusion.1
  452.3 1.9 pad_maximum_fusion.1
  454.3 0.0 all-gather.36.cloned.1.call-start
  454.4 33.7 %reduce-scatter.6.cloned.1.call-done = f32[48,2048]{1,0:T(8,128)} async-done(((f32[384,2048]{1,0:T(8,128)}), f32[48,2048]{1,0:T(8,128)}) %reduce-scatter.6.cloned.1.call-update) | async-done | bytes 393232 | tf_op jit(solution)/shard_map/reduce_scatter | solution.py:38
  488.1 0.0 all-gather.24.cloned.1.call-start
  488.1 31.5 %all-gather.36.cloned.1.call-done = f32[384,2048]{1,0:T(8,128)} async-done(((f32[48,2048]{1,0:T(8,128)}), f32[384,2048]{1,0:T(8,128)}) %all-gather.36.cloned.1.call-update) | async-done | bytes 3145744 | tf_op jit(solution)/shard_map/all_gather | solution.py:41
  519.6 1.8 constant_dynamic-slice_fusion.1
  521.4 0.0 all-gather.26.cloned.1.call-start
  521.4 61.7 %all-gather.24.cloned.1.call-done = f32[3,2048,256]{2,1,0:T(8,128)} async-done(((f32[3,128,256]{2,1,0:T(8,128)}), f32[3,2048,256]{2,1,0:T(8,128)}) %all-gather.24.cloned.1.call-update) | async-done | bytes 6291472 | tf_op jit(solution)/shard_map/all_gather | solution.py:78
  583.1 8.2 fusion.11
  591.3 0.4 all-gather.28.cloned.1.call-start
  591.8 27.5 %all-gather.26.cloned.1.call-done = f32[3,128,2048]{2,1,0:T(8,128)} async-done(((f32[3,128,256]{2,1,0:T(8,128)}), f32[3,128,2048]{2,1,0:T(8,128)}) %all-gather.26.cloned.1.call-update) | async-done | bytes 3145744 | tf_op jit(solution)/shard_map/all_gather | solution.py:81
  619.3 4.1 fusion.19
  623.4 0.1 copy.14
  623.5 13.0 %convolution_add_fusion.1 = f32[2,128,704]{1,2,0:T(8,128)S(1)} fusion(f32[3,128,2048]{2,1,0:T(8,128)} %all-gather.26.cloned.1.call-done, f32[2,2048,704]{1,2,0:T(8,128)} %bitcast.69, f32[2,128,704]{1,2,0:T(8,128)S(1)} %fusion.9), kind=kOutput, calls=%fused_computation.16 | convolution fusion | flops 4429545472 | bytes 16121856 | tf_op jit(solution)/shard_map/krs,ksc->krc/dot_general | solution.py:83
  636.5 1.0 pad_maximum_fusion.5
  637.5 0.0 reduce-scatter.8.cloned.1.call-start
  637.6 102.3 %all-gather.28.cloned.1.call-done = f32[2048,1664]{0,1:T(8,128)} async-done(((f32[128,1664]{0,1:T(8,128)}), f32[2048,1664]{0,1:T(8,128)}) %all-gather.28.cloned.1.call-update) | async-done | bytes 13631504 | tf_op jit(solution)/shard_map/all_gather | solution.py:21
  739.8 10.4 %slice.64 = f32[2048,1408]{0,1:T(8,128)} slice(f32[2048,1664]{0,1:T(8,128)} %all-gather.28.cloned.1.call-done), slice={[0:2048], [0:1408]} | slice | bytes 23068672 | tf_op jit(solution)/shard_map/slice | solution.py:23
  750.2 9.2 fusion.27
  759.4 2.8 convolution_bitcast_fusion
  762.2 1.9 pad_maximum_fusion.2
  764.2 0.0 all-gather.38.cloned.1.call-start
  764.2 33.7 %reduce-scatter.8.cloned.1.call-done = f32[48,2048]{1,0:T(8,128)} async-done(((f32[384,2048]{1,0:T(8,128)}), f32[48,2048]{1,0:T(8,128)}) %reduce-scatter.8.cloned.1.call-update) | async-done | bytes 393232 | tf_op jit(solution)/shard_map/reduce_scatter | solution.py:38
  797.9 0.0 all-gather.30.cloned.1.call-start
  798.0 31.5 %all-gather.38.cloned.1.call-done = f32[384,2048]{1,0:T(8,128)} async-done(((f32[48,2048]{1,0:T(8,128)}), f32[384,2048]{1,0:T(8,128)}) %all-gather.38.cloned.1.call-update) | async-done | bytes 3145744 | tf_op jit(solution)/shard_map/all_gather | solution.py:41
  829.5 1.8 constant_dynamic-slice_fusion
  831.3 0.2 all-gather.32.cloned.1.call-start
  831.5 61.4 %all-gather.30.cloned.1.call-done = f32[3,2048,256]{2,1,0:T(8,128)} async-done(((f32[3,128,256]{2,1,0:T(8,128)}), f32[3,2048,256]{2,1,0:T(8,128)}) %all-gather.30.cloned.1.call-update) | async-done | bytes 6291472 | tf_op jit(solution)/shard_map/all_gather | solution.py:78
  892.8 8.2 fusion.12
  901.1 27.9 %all-gather.32.cloned.1.call-done = f32[3,128,2048]{2,1,0:T(8,128)} async-done(((f32[3,128,256]{2,1,0:T(8,128)}), f32[3,128,2048]{2,1,0:T(8,128)}) %all-gather.32.cloned.1.call-update) | async-done | bytes 3145744 | tf_op jit(solution)/shard_map/all_gather | solution.py:81
  929.0 5.0 broadcast_multiply_fusion.1
  934.0 13.9 %broadcast_multiply_fusion = (f32[2,128,704]{1,2,0:T(8,128)}, f32[2,128,704]{1,2,0:T(8,128)}) fusion(f32[2,128,704]{1,2,0:T(8,128)S(1)} %copy-done.3, f32[3,128,2048]{2,1,0:T(8,128)S(1)} %copy-done.1, f32[2,2048,704]{1,2,0:T(8,128)} %bitcast.67, f32[2,128,704]{1,2,0:T(8,128)S(1)} %convolution_add_fusion.1), kind=kOutput, calls=%fused_computation.38 | convolution fusion | flops 4430086144 | bytes 17563648 | tf_op jit(solution)/shard_map/krs,ksc->krc/dot_general | solution.py:83
  (30 shorter events, 0.3 us)
Async XLA Ops:
  7.2 109.6 %all-gather.16.cloned.1.call-start = ((), (), s32[]{:S(2)}) async-start(), calls=%async_computation.3 | async-start | bytes 14483456 | tf_op jit(solution)/shard_map/all_gather | solution.py:21
  8.2 300.5 %copy-start.2 = (f32[128,256]{1,0:T(8,128)}, f32[128,256]{1,0:T(8,128)S(1)}, u32[]{:S(2)}) copy-start(f32[128,256]{1,0:T(8,128)S(1)} %multiply_add_fusion.1) | copy-start | bytes 393220
  9.7 303.9 %copy-start = (f32[2,128,704]{1,2,0:T(8,128)}, f32[2,128,704]{1,2,0:T(8,128)S(1)}, u32[]{:S(2)}) copy-start(f32[2,128,704]{1,2,0:T(8,128)S(1)} %multiply_add_fusion) | copy-start | bytes 2162692
  10.8 164.1 %reduce-scatter.4.cloned.1.call-start = ((), (), s32[]{:S(2)}) async-start(), calls=%async_computation.4 | async-start | bytes 3538944 | tf_op jit(solution)/shard_map/reduce_scatter | solution.py:38
  141.2 65.3 %all-gather.34.cloned.1.call-start = ((), (), s32[]{:S(2)}) async-start(), calls=%async_computation.15 | async-start | bytes 3538944 | tf_op jit(solution)/shard_map/all_gather | solution.py:41
  174.9 100.9 %all-gather.18.cloned.1.call-start = ((), (), s32[]{:S(2)}) async-start(), calls=%async_computation.5 | async-start | bytes 6684672 | tf_op jit(solution)/shard_map/all_gather | solution.py:78
  208.2 100.5 %all-gather.20.cloned.1.call-start = ((), (), s32[]{:S(2)}) async-start(), calls=%async_computation.6 | async-start | bytes 3538944 | tf_op jit(solution)/shard_map/all_gather | solution.py:81
  284.1 145.9 %all-gather.22.cloned.1.call-start = ((), (), s32[]{:S(2)}) async-start(), calls=%async_computation.7 | async-start | bytes 14483456 | tf_op jit(solution)/shard_map/all_gather | solution.py:21
  327.6 160.4 %reduce-scatter.6.cloned.1.call-start = ((), (), s32[]{:S(2)}) async-start(), calls=%async_computation.8 | async-start | bytes 3538944 | tf_op jit(solution)/shard_map/reduce_scatter | solution.py:38
  454.3 65.3 %all-gather.36.cloned.1.call-start = ((), (), s32[]{:S(2)}) async-start(), calls=%async_computation.16 | async-start | bytes 3538944 | tf_op jit(solution)/shard_map/all_gather | solution.py:41
  488.1 95.1 %all-gather.24.cloned.1.call-start = ((), (), s32[]{:S(2)}) async-start(), calls=%async_computation.9 | async-start | bytes 6684672 | tf_op jit(solution)/shard_map/all_gather | solution.py:78
  521.4 97.9 %all-gather.26.cloned.1.call-start = ((), (), s32[]{:S(2)}) async-start(), calls=%async_computation.10 | async-start | bytes 3538944 | tf_op jit(solution)/shard_map/all_gather | solution.py:81
  591.3 148.5 %all-gather.28.cloned.1.call-start = ((), (), s32[]{:S(2)}) async-start(), calls=%async_computation.11 | async-start | bytes 14483456 | tf_op jit(solution)/shard_map/all_gather | solution.py:21
  637.5 160.4 %reduce-scatter.8.cloned.1.call-start = ((), (), s32[]{:S(2)}) async-start(), calls=%async_computation.12 | async-start | bytes 3538944 | tf_op jit(solution)/shard_map/reduce_scatter | solution.py:38
  764.2 65.3 %all-gather.38.cloned.1.call-start = ((), (), s32[]{:S(2)}) async-start(), calls=%async_computation.17 | async-start | bytes 3538944 | tf_op jit(solution)/shard_map/all_gather | solution.py:41
  797.9 94.9 %all-gather.30.cloned.1.call-start = ((), (), s32[]{:S(2)}) async-start(), calls=%async_computation.13 | async-start | bytes 6684672 | tf_op jit(solution)/shard_map/all_gather | solution.py:78
  831.2 97.8 %copy-start.4 = (f32[128,256]{1,0:T(8,128)S(1)}, f32[128,256]{1,0:T(8,128)}, u32[]{:S(2)}) copy-start(f32[128,256]{1,0:T(8,128)} %param.7) | copy-start | bytes 393220
  831.3 97.8 %all-gather.32.cloned.1.call-start = ((), (), s32[]{:S(2)}) async-start(), calls=%async_computation.14 | async-start | bytes 3538944 | tf_op jit(solution)/shard_map/all_gather | solution.py:81
  901.1 33.0 %copy-start.3 = (f32[2,128,704]{1,2,0:T(8,128)S(1)}, f32[2,128,704]{1,2,0:T(8,128)}, u32[]{:S(2)}) copy-start(f32[2,128,704]{1,2,0:T(8,128)} %param.6) | copy-start | bytes 2162692
  929.0 5.0 copy-start.1
Sparse Core Ops, SparseCore 0:
  10.9 105.7 all-gather.15
  141.3 33.5 reduce-scatter.3
  176.6 29.8 all-gather.33
  209.0 61.3 all-gather.17
  284.2 24.4 all-gather.19
  327.7 102.1 all-gather.21
  454.4 33.5 reduce-scatter.5
  489.7 29.8 all-gather.35
  522.3 60.7 all-gather.23
  591.5 27.7 all-gather.25
  637.6 102.1 all-gather.27
  764.3 33.5 reduce-scatter.7
  799.6 29.8 all-gather.37
  832.0 60.7 all-gather.29
  901.2 27.7 all-gather.31
where the time goes:
time: 963 us; the launch traced here: 955 us
  waiting for transfers between devices  708 us (74%)
  matrix products  114 us (12%)
  blocking collectives  67.5 us (7%)
  local copies, waits for them, and re-layouts  35.7 us (4%)
  between operations  14.3 us (1%)
  other arithmetic  13.1 us (1%)
    all_gather x3, waiting for transfers between devices, gather_turned(): lax.all_gather(both, axis, axis=0, tiled=True)  310 us
    all_gather x3, waiting for transfers between devices, local(): gram_cols = lax.all_gather(gram_block, 'fs', axis=1, tiled=True)  123 us
    reduce_scatter x3, waiting for transfers between devices, sum_by_parts(): lax.psum_scatter(rows_for(lines, lax.axis_size(axis)), axis, scatter_dime...  101 us
    all_gather x3, waiting for transfers between devices, sum_by_parts(): whole = lax.all_gather(own, axis).reshape(-1, *lines.shape[1:])  94.3 us
    all_gather x3, waiting for transfers between devices, local(): poly_rows = lax.all_gather(poly_mat, 'tp', axis=2, tiled=True)  79.3 us
    psum x1, blocking collectives, local(): scaling = scale_from(lax.psum(traces, ('fs', 'tp')))  67.5 us
    dot_general x3, matrix products, local(): jnp.einsum('krs,ksc->krc', poly_rows[:2], cols_in, precision=HIGH)  39.9 us
    slice x3, local copies, waits for them, and re-layouts, gather_turned(): share = result[:, at:at + t[0].size].reshape(-1, *t.shape[1:])  31.2 us
  transfers between devices with their start and end apart: 15, of which 14 were waited for; matrix products, arithmetic and copies ran while one was open for 0% of the time, Pallas kernels for 0%

commit v1 on v0

--- a/solution.py
+++ b/solution.py
@@ -73,7 +73,7 @@
         gram_block = lax.dynamic_slice_in_dim(gram_rows, tp_pos * block_width, block_width, 2)
         if iteration == 0:
             traces = block_trace(gram_block, fs_pos * row_count, tp_pos * block_width)
-            scaling = scale_from(lax.psum(traces, ("fs", "tp")))
+            scaling = scale_from(jnp.sum(lax.all_gather(traces, ("fs", "tp")), axis=0))
         factor = scaling if iteration == 0 else jnp.ones_like(scaling)
         gram_cols = lax.all_gather(gram_block, "fs", axis=1, tiled=True)
         square = jnp.einsum("krs,ksc->krc", gram_rows, gram_cols, precision=HIGH)

time: 963 us -> 964 us (level)
    unnamed x0 -> x1, blocking collectives: none -> 67.6 us
    psum x1 -> x0, blocking collectives: 67.5 us -> none  [local(): scaling = scale_from(lax.psum(traces, ('fs', 'tp')))]
where the time goes in v1:
time: 964 us; the launch traced here: 955 us
  waiting for transfers between devices  708 us (73%)
  matrix products  114 us (12%)
  blocking collectives  67.6 us (7%)
  local copies, waits for them, and re-layouts  36.1 us (4%)
  between operations  14.3 us (1%)
  other arithmetic  13.2 us (1%)
    all_gather x3, waiting for transfers between devices, gather_turned(): lax.all_gather(both, axis, axis=0, tiled=True)  310 us
    all_gather x3, waiting for transfers between devices, local(): gram_cols = lax.all_gather(gram_block, 'fs', axis=1, tiled=True)  123 us
    reduce_scatter x3, waiting for transfers between devices, sum_by_parts(): lax.psum_scatter(rows_for(lines, lax.axis_size(axis)), axis, scatter_dime...  101 us
    all_gather x3, waiting for transfers between devices, sum_by_parts(): whole = lax.all_gather(own, axis).reshape(-1, *lines.shape[1:])  94.3 us
    all_gather x3, waiting for transfers between devices, local(): poly_rows = lax.all_gather(poly_mat, 'tp', axis=2, tiled=True)  79.2 us
    unnamed x1, blocking collectives  67.6 us
    dot_general x3, matrix products, local(): jnp.einsum('krs,ksc->krc', poly_rows[:2], cols_in, precision=HIGH)  39.9 us
    slice x3, local copies, waits for them, and re-layouts, gather_turned(): share = result[:, at:at + t[0].size].reshape(-1, *t.shape[1:])  31.2 us
  transfers between devices with their start and end apart: 15, of which 14 were waited for; matrix products, arithmetic and copies ran while one was open for 0% of the time, Pallas kernels for 0%

profile of v1, /device:TPU:1, one launch (start us, length us, event | category | flops | bytes accessed | tf_op | source)
XLA Modules:
  0.0 955.2 jit_solution(2922891535875609359)
XLA Ops:
  7.2 1.0 multiply_add_fusion.1
  8.2 0.1 copy.15
  8.3 1.4 multiply_add_fusion
  9.7 1.1 pad_maximum_fusion.3
  10.8 0.0 reduce-scatter.4.cloned.1.call-start
  10.9 105.9 %all-gather.17.cloned.1.call-done = f32[2048,1664]{0,1:T(8,128)} async-done(((f32[128,1664]{0,1:T(8,128)}), f32[2048,1664]{0,1:T(8,128)}) %all-gather.17.cloned.1.call-update) | async-done | bytes 13631504 | tf_op jit(solution)/shard_map/all_gather | solution.py:21
  116.8 10.4 %slice.58 = f32[2048,1408]{0,1:T(8,128)} slice(f32[2048,1664]{0,1:T(8,128)} %all-gather.17.cloned.1.call-done), slice={[0:2048], [0:1408]} | slice | bytes 23068672 | tf_op jit(solution)/shard_map/slice | solution.py:23
  127.2 9.2 fusion.25
  136.4 2.8 convolution_bitcast_fusion.2
  139.2 1.9 pad_maximum_fusion
  141.2 0.0 all-gather.35.cloned.1.call-start
  141.2 33.6 %reduce-scatter.4.cloned.1.call-done = f32[48,2048]{1,0:T(8,128)} async-done(((f32[384,2048]{1,0:T(8,128)}), f32[48,2048]{1,0:T(8,128)}) %reduce-scatter.4.cloned.1.call-update) | async-done | bytes 393232 | tf_op jit(solution)/shard_map/reduce_scatter | solution.py:38
  174.9 0.0 all-gather.19.cloned.1.call-start
  174.9 0.1 broadcast_compare_fusion
  175.0 31.4 %all-gather.35.cloned.1.call-done = f32[384,2048]{1,0:T(8,128)} async-done(((f32[48,2048]{1,0:T(8,128)}), f32[384,2048]{1,0:T(8,128)}) %all-gather.35.cloned.1.call-update) | async-done | bytes 3145744 | tf_op jit(solution)/shard_map/all_gather | solution.py:41
  206.4 1.8 select_reduce_fusion
  208.2 0.0 all-gather.21.cloned.1.call-start
  208.3 0.2 dynamic-update-slice
  208.5 67.6 %all-reduce = f32[384]{0:T(512)S(1)} all-reduce(f32[384]{0:T(512)S(1)} %dynamic-update-slice), channel_id=3, replica_groups=mesh['fs'=16,'tp'=8] {'fs','tp'}, use_global_device_ids=true, to_apply=%add | all-reduce | flops 384 | bytes 3072
  276.1 0.2 reshape.154
  276.4 8.2 fusion.10
  284.6 0.2 all-gather.23.cloned.1.call-start
  284.9 0.6 slice.48
  285.4 23.8 %all-gather.21.cloned.1.call-done = f32[3,128,2048]{2,1,0:T(8,128)} async-done(((f32[3,128,256]{2,1,0:T(8,128)}), f32[3,128,2048]{2,1,0:T(8,128)}) %all-gather.21.cloned.1.call-update) | async-done | bytes 3145744 | tf_op jit(solution)/shard_map/all_gather | solution.py:81
  309.2 4.8 fusion.16
  314.0 0.1 copy.16
  314.1 13.0 %fusion.9 = f32[2,128,704]{1,2,0:T(8,128)S(1)} fusion(f32[3,128,2048]{2,1,0:T(8,128)} %all-gather.21.cloned.1.call-done, f32[2,2048,704]{1,2,0:T(8,128)} %bitcast.65, f32[2,128,704]{1,2,0:T(8,128)S(1)} %multiply_add_fusion, f32[2]{0:T(128)S(1)} %bitcast.82), kind=kOutput, calls=%fused_computation.18 | convolution fusion | flops 4429725696 | bytes 16121864 | tf_op jit(solution)/shard_map/krs,ksc->krc/dot_general | solution.py:83
  327.1 1.0 pad_maximum_fusion.4
  328.2 0.3 reduce-scatter.6.cloned.1.call-start
  328.4 102.1 %all-gather.23.cloned.1.call-done = f32[2048,1664]{0,1:T(8,128)} async-done(((f32[128,1664]{0,1:T(8,128)}), f32[2048,1664]{0,1:T(8,128)}) %all-gather.23.cloned.1.call-update) | async-done | bytes 13631504 | tf_op jit(solution)/shard_map/all_gather | solution.py:21
  430.5 10.4 %slice.61 = f32[2048,1408]{0,1:T(8,128)} slice(f32[2048,1664]{0,1:T(8,128)} %all-gather.23.cloned.1.call-done), slice={[0:2048], [0:1408]} | slice | bytes 23068672 | tf_op jit(solution)/shard_map/slice | solution.py:23
  440.9 9.2 fusion.26
  450.1 2.8 convolution_bitcast_fusion.1
  452.9 1.9 pad_maximum_fusion.1
  454.9 0.0 all-gather.37.cloned.1.call-start
  454.9 33.6 %reduce-scatter.6.cloned.1.call-done = f32[48,2048]{1,0:T(8,128)} async-done(((f32[384,2048]{1,0:T(8,128)}), f32[48,2048]{1,0:T(8,128)}) %reduce-scatter.6.cloned.1.call-update) | async-done | bytes 393232 | tf_op jit(solution)/shard_map/reduce_scatter | solution.py:38
  488.6 0.0 all-gather.25.cloned.1.call-start
  488.6 31.5 %all-gather.37.cloned.1.call-done = f32[384,2048]{1,0:T(8,128)} async-done(((f32[48,2048]{1,0:T(8,128)}), f32[384,2048]{1,0:T(8,128)}) %all-gather.37.cloned.1.call-update) | async-done | bytes 3145744 | tf_op jit(solution)/shard_map/all_gather | solution.py:41
  520.1 1.8 constant_dynamic-slice_fusion.1
  521.9 0.0 all-gather.27.cloned.1.call-start
  521.9 61.7 %all-gather.25.cloned.1.call-done = f32[3,2048,256]{2,1,0:T(8,128)} async-done(((f32[3,128,256]{2,1,0:T(8,128)}), f32[3,2048,256]{2,1,0:T(8,128)}) %all-gather.25.cloned.1.call-update) | async-done | bytes 6291472 | tf_op jit(solution)/shard_map/all_gather | solution.py:78
  583.7 8.2 fusion.11
  591.9 0.4 all-gather.29.cloned.1.call-start
  592.3 27.5 %all-gather.27.cloned.1.call-done = f32[3,128,2048]{2,1,0:T(8,128)} async-done(((f32[3,128,256]{2,1,0:T(8,128)}), f32[3,128,2048]{2,1,0:T(8,128)}) %all-gather.27.cloned.1.call-update) | async-done | bytes 3145744 | tf_op jit(solution)/shard_map/all_gather | solution.py:81
  619.8 4.1 fusion.19
  624.0 0.1 copy.17
  624.1 13.0 %convolution_add_fusion.1 = f32[2,128,704]{1,2,0:T(8,128)S(1)} fusion(f32[3,128,2048]{2,1,0:T(8,128)} %all-gather.27.cloned.1.call-done, f32[2,2048,704]{1,2,0:T(8,128)} %bitcast.69, f32[2,128,704]{1,2,0:T(8,128)S(1)} %fusion.9), kind=kOutput, calls=%fused_computation.16 | convolution fusion | flops 4429545472 | bytes 16121856 | tf_op jit(solution)/shard_map/krs,ksc->krc/dot_general | solution.py:83
  637.1 1.0 pad_maximum_fusion.5
  638.1 0.0 reduce-scatter.8.cloned.1.call-start
  638.1 102.3 %all-gather.29.cloned.1.call-done = f32[2048,1664]{0,1:T(8,128)} async-done(((f32[128,1664]{0,1:T(8,128)}), f32[2048,1664]{0,1:T(8,128)}) %all-gather.29.cloned.1.call-update) | async-done | bytes 13631504 | tf_op jit(solution)/shard_map/all_gather | solution.py:21
  740.4 10.4 %slice.64 = f32[2048,1408]{0,1:T(8,128)} slice(f32[2048,1664]{0,1:T(8,128)} %all-gather.29.cloned.1.call-done), slice={[0:2048], [0:1408]} | slice | bytes 23068672 | tf_op jit(solution)/shard_map/slice | solution.py:23
  750.8 9.2 fusion.27
  760.0 2.8 convolution_bitcast_fusion
  762.8 1.9 pad_maximum_fusion.2
  764.8 0.0 all-gather.39.cloned.1.call-start
  764.8 33.6 %reduce-scatter.8.cloned.1.call-done = f32[48,2048]{1,0:T(8,128)} async-done(((f32[384,2048]{1,0:T(8,128)}), f32[48,2048]{1,0:T(8,128)}) %reduce-scatter.8.cloned.1.call-update) | async-done | bytes 393232 | tf_op jit(solution)/shard_map/reduce_scatter | solution.py:38
  798.5 31.5 %all-gather.39.cloned.1.call-done = f32[384,2048]{1,0:T(8,128)} async-done(((f32[48,2048]{1,0:T(8,128)}), f32[384,2048]{1,0:T(8,128)}) %all-gather.39.cloned.1.call-update) | async-done | bytes 3145744 | tf_op jit(solution)/shard_map/all_gather | solution.py:41
  830.0 1.8 constant_dynamic-slice_fusion
  831.8 0.2 all-gather.33.cloned.1.call-start
  832.0 61.4 %all-gather.31.cloned.1.call-done = f32[3,2048,256]{2,1,0:T(8,128)} async-done(((f32[3,128,256]{2,1,0:T(8,128)}), f32[3,2048,256]{2,1,0:T(8,128)}) %all-gather.31.cloned.1.call-update) | async-done | bytes 6291472 | tf_op jit(solution)/shard_map/all_gather | solution.py:78
  893.4 8.2 fusion.12
  901.7 27.9 %all-gather.33.cloned.1.call-done = f32[3,128,2048]{2,1,0:T(8,128)} async-done(((f32[3,128,256]{2,1,0:T(8,128)}), f32[3,128,2048]{2,1,0:T(8,128)}) %all-gather.33.cloned.1.call-update) | async-done | bytes 3145744 | tf_op jit(solution)/shard_map/all_gather | solution.py:81
  929.6 5.0 broadcast_multiply_fusion.1
  934.6 13.9 %broadcast_multiply_fusion = (f32[2,128,704]{1,2,0:T(8,128)}, f32[2,128,704]{1,2,0:T(8,128)}) fusion(f32[2,128,704]{1,2,0:T(8,128)S(1)} %copy-done.3, f32[3,128,2048]{2,1,0:T(8,128)S(1)} %copy-done.1, f32[2,2048,704]{1,2,0:T(8,128)} %bitcast.67, f32[2,128,704]{1,2,0:T(8,128)S(1)} %convolution_add_fusion.1), kind=kOutput, calls=%fused_computation.38 | convolution fusion | flops 4430086144 | bytes 17563648 | tf_op jit(solution)/shard_map/krs,ksc->krc/dot_general | solution.py:83
  (34 shorter events, 0.4 us)
Async XLA Ops:
  7.2 109.6 %all-gather.17.cloned.1.call-start = ((), (), s32[]{:S(2)}) async-start(), calls=%async_computation.3 | async-start | bytes 14483456 | tf_op jit(solution)/shard_map/all_gather | solution.py:21
  8.2 301.0 %copy-start.2 = (f32[128,256]{1,0:T(8,128)}, f32[128,256]{1,0:T(8,128)S(1)}, u32[]{:S(2)}) copy-start(f32[128,256]{1,0:T(8,128)S(1)} %multiply_add_fusion.1) | copy-start | bytes 393220
  9.7 304.4 %copy-start = (f32[2,128,704]{1,2,0:T(8,128)}, f32[2,128,704]{1,2,0:T(8,128)S(1)}, u32[]{:S(2)}) copy-start(f32[2,128,704]{1,2,0:T(8,128)S(1)} %multiply_add_fusion) | copy-start | bytes 2162692
  10.8 164.0 %reduce-scatter.4.cloned.1.call-start = ((), (), s32[]{:S(2)}) async-start(), calls=%async_computation.4 | async-start | bytes 3538944 | tf_op jit(solution)/shard_map/reduce_scatter | solution.py:38
  141.2 65.3 %all-gather.35.cloned.1.call-start = ((), (), s32[]{:S(2)}) async-start(), calls=%async_computation.15 | async-start | bytes 3538944 | tf_op jit(solution)/shard_map/all_gather | solution.py:41
  174.9 101.5 %all-gather.19.cloned.1.call-start = ((), (), s32[]{:S(2)}) async-start(), calls=%async_computation.5 | async-start | bytes 6684672 | tf_op jit(solution)/shard_map/all_gather | solution.py:78
  208.2 101.0 %all-gather.21.cloned.1.call-start = ((), (), s32[]{:S(2)}) async-start(), calls=%async_computation.6 | async-start | bytes 3538944 | tf_op jit(solution)/shard_map/all_gather | solution.py:81
  284.6 145.8 %all-gather.23.cloned.1.call-start = ((), (), s32[]{:S(2)}) async-start(), calls=%async_computation.7 | async-start | bytes 14483456 | tf_op jit(solution)/shard_map/all_gather | solution.py:21
  328.2 160.4 %reduce-scatter.6.cloned.1.call-start = ((), (), s32[]{:S(2)}) async-start(), calls=%async_computation.8 | async-start | bytes 3538944 | tf_op jit(solution)/shard_map/reduce_scatter | solution.py:38
  454.9 65.2 %all-gather.37.cloned.1.call-start = ((), (), s32[]{:S(2)}) async-start(), calls=%async_computation.16 | async-start | bytes 3538944 | tf_op jit(solution)/shard_map/all_gather | solution.py:41
  488.6 95.1 %all-gather.25.cloned.1.call-start = ((), (), s32[]{:S(2)}) async-start(), calls=%async_computation.9 | async-start | bytes 6684672 | tf_op jit(solution)/shard_map/all_gather | solution.py:78
  521.9 97.9 %all-gather.27.cloned.1.call-start = ((), (), s32[]{:S(2)}) async-start(), calls=%async_computation.10 | async-start | bytes 3538944 | tf_op jit(solution)/shard_map/all_gather | solution.py:81
  591.9 148.5 %all-gather.29.cloned.1.call-start = ((), (), s32[]{:S(2)}) async-start(), calls=%async_computation.11 | async-start | bytes 14483456 | tf_op jit(solution)/shard_map/all_gather | solution.py:21
  638.1 160.4 %reduce-scatter.8.cloned.1.call-start = ((), (), s32[]{:S(2)}) async-start(), calls=%async_computation.12 | async-start | bytes 3538944 | tf_op jit(solution)/shard_map/reduce_scatter | solution.py:38
  764.8 65.2 %all-gather.39.cloned.1.call-start = ((), (), s32[]{:S(2)}) async-start(), calls=%async_computation.17 | async-start | bytes 3538944 | tf_op jit(solution)/shard_map/all_gather | solution.py:41
  798.5 94.9 %all-gather.31.cloned.1.call-start = ((), (), s32[]{:S(2)}) async-start(), calls=%async_computation.13 | async-start | bytes 6684672 | tf_op jit(solution)/shard_map/all_gather | solution.py:78
  831.8 97.8 %copy-start.4 = (f32[128,256]{1,0:T(8,128)S(1)}, f32[128,256]{1,0:T(8,128)}, u32[]{:S(2)}) copy-start(f32[128,256]{1,0:T(8,128)} %param.7) | copy-start | bytes 393220
  831.8 97.8 %all-gather.33.cloned.1.call-start = ((), (), s32[]{:S(2)}) async-start(), calls=%async_computation.14 | async-start | bytes 3538944 | tf_op jit(solution)/shard_map/all_gather | solution.py:81
  901.6 33.0 %copy-start.3 = (f32[2,128,704]{1,2,0:T(8,128)S(1)}, f32[2,128,704]{1,2,0:T(8,128)}, u32[]{:S(2)}) copy-start(f32[2,128,704]{1,2,0:T(8,128)} %param.6) | copy-start | bytes 2162692
  929.6 5.0 copy-start.1
Sparse Core Ops, SparseCore 0:
  10.9 105.7 all-gather.16
  141.3 33.5 reduce-scatter.3
  176.5 29.8 all-gather.34
  209.0 61.2 all-gather.18
  284.8 24.4 all-gather.20
  328.3 102.1 all-gather.22
  455.0 33.5 reduce-scatter.5
  490.2 29.8 all-gather.36
  522.8 60.7 all-gather.24
  592.0 27.7 all-gather.26
  638.2 102.1 all-gather.28
  764.9 33.5 reduce-scatter.7
  800.1 29.8 all-gather.38
  832.6 60.7 all-gather.30
  901.8 27.7 all-gather.32
